TPU v7x, 32 devices: a whole 2x2x4 slice. The times are simulated.
32 devices in a mesh: sp: 16 (over z, y, x), tp: 2 (over core).
Axes of the slice: x: 2, y: 2, z: 4, core: 2. Of those that a mesh axis runs over, the one named last changes fastest.
Arguments:
- query_small: bfloat16 [6144, 2, 128], P('sp', 'tp'), may hold values from -8 to 8
- key_small: bfloat16 [6144, 2, 128], P('sp', 'tp'), may hold values from -8 to 8
- value_small: bfloat16 [6144, 2, 128], P('sp', 'tp'), may hold values from -6 to 6
- query_large: bfloat16 [6144, 2, 256], P('sp', 'tp'), may hold values from -8 to 8
- key_large: bfloat16 [6144, 2, 256], P('sp', 'tp'), may hold values from -8 to 8
- value_large: bfloat16 [6144, 2, 128], P('sp', 'tp'), may hold values from -6 to 6
- lambdas: float32 [2, 2], P('tp'), may hold values from 0.3 to 0.8
- slopes: float32 [2, 2], P('tp'), as said below
- head_gain: bfloat16 [128], replicated, may hold values from 0.099609375 to 1.8984375
- residual: bfloat16 [6144, 2048], P(('sp', 'tp')), may hold values from -6 to 6
- out_weight: bfloat16 [512, 2048], replicated, may hold values from -0.25 to 0.25
- norm_gains: bfloat16 [2, 2048], replicated, may hold values from 0.099609375 to 1.8984375
- routes: int32 [6144, 2], P(('sp', 'tp')), may hold values from 0 to 15, as said below
- route_weights: float32 [6144, 2], P(('sp', 'tp')), may hold values from 0.1 to 1
- gate_weight: bfloat16 [16, 2048, 1024], P('sp', None, 'tp'), may hold values from -0.125 to 0.125
- up_weight: bfloat16 [16, 2048, 1024], P('sp', None, 'tp'), may hold values from -0.125 to 0.125
- down_weight: bfloat16 [16, 1024, 2048], P('sp', 'tp'), may hold values from -0.1875 to 0.1875
Outputs:
- layer_out: bfloat16 [6144, 2048], P(('sp', 'tp'))
Inputs may be any that keep to these rules, and one draw needn't show every extreme that they name: `slopes`: positive. `routes`: each token names two different experts of one group of 4 consecutive expert numbers. In each aligned block of 192 rows (the tokens of one device) no expert is named more than 48 times, and some expert is named exactly 48 times in every block.
All inputs are finite; a program needn't handle non-finite values.
Results may differ from a plain program's by a relative error of at most 0.011.
Values may be sent and summed in bfloat16 or wider, within the bound.
A program may use at most 128 MiB of HBM per device.

v0:
```python
import math

import jax
import jax.numpy as jnp
from jax import lax
from jax.sharding import PartitionSpec as P

residual_gain = 8.0**0.25
epsilon = 1e-05
masked_score = -1e30


def layer_norm(values, gain_row):
    average = jnp.mean(values, axis=-1, keepdims=True)
    centred = values - average
    variance = jnp.mean(centred * centred, axis=-1, keepdims=True)
    return centred * lax.rsqrt(variance + epsilon) * gain_row.astype(jnp.float32)


def empty_state(head_count, length, value_size):
    return (
        jnp.full((head_count, 2, length), masked_score, jnp.float32),
        jnp.zeros((head_count, 2, length), jnp.float32),
        jnp.zeros((head_count, 2, length, value_size), jnp.float32),
    )


def advance(carried, keyset, valueset, queries, slope_row, positions):
    head_count = queries.shape[1]
    key_width = queries.shape[3]
    length = keyset.shape[0]
    block_rows = math.gcd(length, 512)
    blocks = length // block_rows
    key_blocks = keyset.reshape(blocks, block_rows, head_count, 2, key_width)
    value_blocks = valueset.reshape(blocks, block_rows, head_count, -1)
    score_scale = key_width ** (-0.5)
    last_query = positions[-1]

    def update(running, inputs):
        key_block, value_block, number = inputs
        first_key = number * block_rows

        def compute(current):
            running_max, running_sum, running_acc = current
            scores = (
                jnp.einsum(
                    "qhmd,khmd->hmqk", queries, key_block, preferred_element_type=jnp.float32
                )
                * score_scale
            )
            distance = (positions[:, None] - (first_key + jnp.arange(block_rows))[None, :]).astype(
                jnp.float32
            )
            scores = scores - slope_row[:, None, None, None] * distance
            scores = jnp.where(distance >= 0, scores, masked_score)
            new_max = jnp.maximum(running_max, jnp.max(scores, axis=-1))
            factor = jnp.exp(running_max - new_max)
            weights = jnp.exp(scores - new_max[..., None])
            new_sum = running_sum * factor + jnp.sum(weights, axis=-1)
            product = jnp.einsum(
                "hmqk,khe->hmqe",
                weights.astype(jnp.bfloat16),
                value_block,
                preferred_element_type=jnp.float32,
            )
            return (new_max, new_sum, running_acc * factor[..., None] + product)

        return (lax.cond(first_key <= last_query, compute, lambda current: current, running), None)

    carried, _ = lax.scan(update, carried, (key_blocks, value_blocks, jnp.arange(blocks)))
    return carried


def finish(carried, lambda_row, head_gain):
    running_max, running_sum, running_acc = carried
    mixture = running_acc / running_sum[..., None]
    head_out = mixture[:, 0] - lambda_row[:, None, None] * mixture[:, 1]
    scaled = head_out * lax.rsqrt(jnp.mean(head_out * head_out, axis=-1, keepdims=True) + epsilon)
    scaled = scaled * head_gain.astype(jnp.float32)
    return jnp.transpose(scaled, (1, 0, 2))


def shards(
    query_small,
    key_small,
    value_small,
    query_large,
    key_large,
    value_large,
    lambdas,
    slopes,
    head_gain,
    residual,
    out_weight,
    norm_gains,
    routes,
    route_weights,
    gate_weight,
    up_weight,
    down_weight,
):
    length = query_small.shape[0]
    head_count = query_small.shape[1]
    value_size = value_small.shape[2]
    positions = lax.axis_index("sp") * length + jnp.arange(length)
    small_queries = query_small.reshape(length, head_count, 2, -1)
    large_queries = query_large.reshape(length, head_count, 2, -1)
    small_start = empty_state(head_count, length, value_size)
    large_start = empty_state(head_count, length, value_size)

    def fold_large(carried, pieces):
        return advance(carried, pieces[0], pieces[1], large_queries, slopes[:, 1], positions)

    pieces = (
        lax.all_gather(key_small, "sp", axis=0, tiled=True),
        lax.all_gather(value_small, "sp", axis=0, tiled=True),
        lax.all_gather(key_large, "sp", axis=0, tiled=True),
        lax.all_gather(value_large, "sp", axis=0, tiled=True),
    )
    small_state = advance(small_start, pieces[0], pieces[1], small_queries, slopes[:, 0], positions)
    large_state = fold_large(large_start, (pieces[2], pieces[3]))
    attended = jnp.stack(
        [
            finish(small_state, lambdas[:, 0], head_gain),
            finish(large_state, lambdas[:, 1], head_gain),
        ],
        axis=2,
    ).astype(jnp.bfloat16)
    core_count = lax.axis_size("tp")
    row_count = length // core_count
    flattened = attended.reshape(length, -1)
    width_rows = flattened.shape[1]
    weight_rows = lax.dynamic_slice_in_dim(
        out_weight, lax.axis_index("tp") * width_rows, width_rows, 0
    )
    projected = lax.psum_scatter(
        jnp.dot(flattened, weight_rows, preferred_element_type=jnp.float32).astype(jnp.bfloat16),
        "tp",
        scatter_dimension=0,
        tiled=True,
    ).astype(jnp.float32)
    middle = layer_norm(
        residual_gain * residual.astype(jnp.float32) + projected, norm_gains[0]
    ).astype(jnp.bfloat16)
    experts = lax.axis_size("sp")
    capacity = 4 * row_count // experts
    features = middle.shape[1]
    chosen = routes.reshape(-1)
    matches = (chosen[:, None] == jnp.arange(experts)[None, :]).astype(jnp.int32)
    earlier = jnp.cumsum(matches, axis=0) - matches
    target = chosen * capacity + jnp.sum(earlier * matches, axis=1)
    selector = jnp.any(
        target.reshape(row_count, 2)[None, :, :] == jnp.arange(experts * capacity)[:, None, None],
        axis=2,
    ).astype(jnp.bfloat16)
    outgoing = jnp.dot(selector, middle, preferred_element_type=jnp.float32).astype(jnp.bfloat16)
    outgoing = outgoing.reshape(experts, capacity, features)
    arrived = lax.all_to_all(outgoing, "sp", split_axis=0, concat_axis=0, tiled=True)
    paired = lax.all_gather(arrived, "tp", axis=0, tiled=True).reshape(-1, features)
    gate_in = jnp.dot(paired, gate_weight[0], preferred_element_type=jnp.float32)
    upward = jnp.dot(paired, up_weight[0], preferred_element_type=jnp.float32)
    hidden = (jax.nn.silu(gate_in) * upward).astype(jnp.bfloat16)
    partial_value = jnp.dot(hidden, down_weight[0], preferred_element_type=jnp.float32).astype(
        jnp.bfloat16
    )
    summed = lax.psum_scatter(
        lax.optimization_barrier(partial_value).astype(jnp.float32).astype(jnp.bfloat16),
        "tp",
        scatter_dimension=0,
        tiled=True,
    )
    returned = lax.all_to_all(
        summed.reshape(experts, capacity, features), "sp", split_axis=0, concat_axis=0, tiled=True
    )
    expert_out = returned.reshape(experts * capacity, features)
    picked = jnp.take(expert_out, target, axis=0).reshape(row_count, 2, features)
    moe_sum = jnp.sum(route_weights[:, :, None] * picked.astype(jnp.float32), axis=1)
    return layer_norm(residual_gain * middle.astype(jnp.float32) + moe_sum, norm_gains[1]).astype(
        jnp.bfloat16
    )


def solution(mesh):
    placed = (
        P("sp", "tp", None),
        P("sp", "tp", None),
        P("sp", "tp", None),
        P("sp", "tp", None),
        P("sp", "tp", None),
        P("sp", "tp", None),
        P("tp", None),
        P("tp", None),
        P(),
        P(("sp", "tp"), None),
        P(),
        P(),
        P(("sp", "tp"), None),
        P(("sp", "tp"), None),
        P("sp", None, "tp"),
        P("sp", None, "tp"),
        P("sp", "tp", None),
    )
    return jax.shard_map(
        shards, mesh=mesh, in_specs=placed, out_specs=P(("sp", "tp"), None), check_vma=False
    )
```

profile of v0, /device:TPU:14, one launch (start us, length us, event | category | flops | bytes accessed | tf_op | source)
XLA Modules:
  0.0 584.4 jit_solution(13606083946513967989)
XLA Ops:
  15.6 51.5 %all-gather.6.cloned.1.call-done = bf16[6144,1,128]{2,0,1:T(8,128)(2,1)} async-done(((bf16[384,1,128]{2,0,1:T(8,128)(2,1)}), bf16[6144,1,128]{2,0,1:T(8,128)(2,1)}) %all-gather.6.cloned.1.call-update) | async-done | bytes 1572880 | tf_op jit(solution)/shard_map/all_gather | solution.py:115
  67.1 6.5 %reshape.589 = bf16[12,512,1,2,64]{4,3,1,0,2:T(2,128)(2,1)} reshape(bf16[6144,1,128]{2,0,1:T(8,128)(2,1)} %all-gather.6.cloned.1.call-done) | data formatting | bytes 3145728 | tf_op jit(solution)/shard_map/reshape | solution.py:34
  73.6 8.2 %copy.74 = bf16[12,512,1,2,64]{1,4,3,2,0:T(8,128)(2,1)} copy(bf16[12,512,1,2,64]{4,3,1,0,2:T(2,128)(2,1)} %reshape.589) | data formatting | bytes 3145728
  81.8 44.8 %all-gather.8.cloned.1.call-done = bf16[6144,1,128]{2,0,1:T(8,128)(2,1)} async-done(((bf16[384,1,128]{2,0,1:T(8,128)(2,1)}), bf16[6144,1,128]{2,0,1:T(8,128)(2,1)}) %all-gather.8.cloned.1.call-update) | async-done | bytes 1572880 | tf_op jit(solution)/shard_map/all_gather | solution.py:116
  126.6 49.8 %while.30 = (s32[]{:T(128)}, f32[1,2,384]{2,1,0:T(2,128)S(1)}, f32[1,2,384]{2,1,0:T(2,128)S(1)}, f32[1,2,384,128]{3,2,1,0:T(8,128)S(1)}, s32[12]{0:T(128)S(1)}, ...) while((s32[]{:T(128)}, f32[1,2,384]{2,1,0:T(2,128)S(1)}, ...), condition=%wide.region_5.6_spmd.clone, body=%wide.region_0.5_spmd.clone.sunk | while | flops 155520128 | bytes 7895879 | solution.py:70
  128.6 4.3 conditional.6
  129.7 1.5 fusion.58
  131.4 1.5 fusion.7
  134.9 4.2 conditional.6
  136.0 1.5 fusion.58
  141.2 4.2 conditional.6
  142.2 1.5 fusion.58
  147.5 4.2 conditional.6
  148.5 1.5 fusion.58
  153.7 4.2 conditional.6
  154.8 1.5 fusion.58
  160.0 4.2 conditional.6
  161.0 1.5 fusion.58
  176.6 20.7 %all-gather.10.cloned.1.call-done = bf16[6144,1,256]{2,0,1:T(8,128)(2,1)} async-done(((bf16[384,1,256]{2,0,1:T(8,128)(2,1)}), bf16[6144,1,256]{2,0,1:T(8,128)(2,1)}) %all-gather.10.cloned.1.call-update) | async-done | bytes 3145744 | tf_op jit(solution)/shard_map/all_gather | solution.py:117
  197.4 5.5 reshape.568
  202.9 4.2 copy.77
  207.1 48.2 %all-gather.12.cloned.1.call-done = bf16[6144,1,128]{2,0,1:T(8,128)(2,1)} async-done(((bf16[384,1,128]{2,0,1:T(8,128)(2,1)}), bf16[6144,1,128]{2,0,1:T(8,128)(2,1)}) %all-gather.12.cloned.1.call-update) | async-done | bytes 1572880 | tf_op jit(solution)/shard_map/all_gather | solution.py:118
  255.4 49.8 %while.31 = (s32[]{:T(128)}, f32[1,2,384]{2,1,0:T(2,128)S(1)}, f32[1,2,384]{2,1,0:T(2,128)S(1)}, f32[1,2,384,128]{3,2,1,0:T(8,128)S(1)}, s32[12]{0:T(128)S(1)}, ...) while((s32[]{:T(128)}, f32[1,2,384]{2,1,0:T(2,128)S(1)}, ...), condition=%wide.region_12.13_spmd.clone, body=%wide.region_7.0_spmd.clone.sunk | while | flops 205851776 | bytes 8125255 | solution.py:70
  257.4 4.2 conditional.7
  258.4 1.5 fusion.59
  263.6 4.2 conditional.7
  264.7 1.5 fusion.59
  269.9 4.2 conditional.7
  270.9 1.5 fusion.59
  276.1 4.2 conditional.7
  277.2 1.5 fusion.59
  282.4 4.2 conditional.7
  283.4 1.5 fusion.59
  288.7 4.2 conditional.7
  289.7 1.5 fusion.59
  308.4 1.8 convolution_convert_fusion.2
  312.3 33.5 %reduce-scatter.3.cloned.1.call-done = bf16[192,2048]{1,0:T(8,128)(2,1)} async-done(((bf16[384,2048]{1,0:T(8,128)(2,1)}), bf16[192,2048]{1,0:T(8,128)(2,1)}) %reduce-scatter.3.cloned.1.call-update) | async-done | bytes 786448 | tf_op jit(solution)/shard_map/reduce_scatter | solution.py:136
  345.8 1.6 fusion.37
  349.4 76.4 %all_to_all.10 = bf16[16,48,2048]{2,1,0:T(8,128)(2,1)} all-to-all(bf16[16,48,2048]{2,1,0:T(8,128)(2,1)S(1)} %bitcast.138), channel_id=1, replica_groups=mesh['sp'=16,'tp'=2] {'sp'}, dimensions={0} | all-to-all | bytes 6291456 | tf_op jit(solution)/shard_map/all_to_all | solution.py:158
  426.0 16.9 %all-gather.14.cloned.1.call-done = bf16[32,48,2048]{2,1,0:T(8,128)(2,1)} async-done(((bf16[16,48,2048]{2,1,0:T(8,128)(2,1)}), bf16[32,48,2048]{2,1,0:T(8,128)(2,1)}) %all-gather.14.cloned.1.call-update) | async-done | bytes 6291472 | tf_op jit(solution)/shard_map/all_gather | solution.py:159
  442.9 8.5 %fusion.35 = f32[1536,512]{1,0:T(8,128)} fusion(bf16[1536,2048]{1,0:T(8,128)(2,1)} %bitcast.154, bf16[1,2048,512]{2,1,0:T(8,128)(2,1)} %param.39), kind=kOutput, calls=%fused_computation.58 | convolution fusion | flops 3221225472 | bytes 11534336 | tf_op jit(solution)/shard_map/dot_general | solution.py:160
  451.4 11.7 %convolution_convert_fusion = bf16[1536,2048]{1,0:T(8,128)(2,1)} fusion(bf16[1,512,2048]{2,1,0:T(8,128)(2,1)S(1)} %copy-done, bf16[1536,2048]{1,0:T(8,128)(2,1)} %bitcast.155, f32[1536,512]{1,0:T(8,128)} %fusion.35, bf16[1,2048,512]{2,1,0:T(8,128)(2,1)} %param.40), kind=kOutput, calls=%fused_computation.49 | convolution fusion | flops 6450315264 | bytes 19922944 | tf_op jit(solution)/shard_map/dot_general | solution.py:163
  463.1 16.2 %reduce-scatter.5.cloned.1.call-done = bf16[768,2048]{1,0:T(8,128)(2,1)} async-done(((bf16[1536,2048]{1,0:T(8,128)(2,1)}), bf16[768,2048]{1,0:T(8,128)(2,1)}) %reduce-scatter.5.cloned.1.call-update) | async-done | bytes 3145744 | tf_op jit(solution)/shard_map/reduce_scatter | solution.py:166
  479.4 7.1 %all-to-all-start.1 = ((bf16[16,48,2048]{2,1,0:T(8,128)(2,1)}), bf16[16,48,2048]{2,1,0:T(8,128)(2,1)}, u32[]{:S(2)}, u32[]{:S(2)}) async-start(bf16[16,48,2048]{2,1,0:T(8,128)(2,1)} %bitcast.140), calls=%async_computation.3 | async-start | bytes 6291456 | tf_op jit(solution)/shard_map/all_to_all | solution.py:172
  487.1 69.6 %all-to-all-done.1 = bf16[16,48,2048]{2,1,0:T(8,128)(2,1)} async-done(((bf16[16,48,2048]{2,1,0:T(8,128)(2,1)}), bf16[16,48,2048]{2,1,0:T(8,128)(2,1)}, u32[]{:S(2)}, u32[]{:S(2)}) %all-to-all-start.1) | async-done | bytes 3145760 | tf_op jit(solution)/shard_map/all_to_all | solution.py:172
  556.7 7.3 %gather_fusion = bf16[384,2048]{1,0:T(8,128)(2,1)} fusion(bf16[768,2048]{1,0:T(8,128)(2,1)} %bitcast.42, s32[1024]{0:T(1024)S(1)} %pad_clamp_fusion), kind=kCustom, calls=%fused_computation | custom fusion | bytes 3147264 | tf_op jit(solution)/shard_map/jit(_take)/gather | solution.py:176
  564.0 3.8 gather.7
  567.8 7.7 %multiply_reduce_fusion = f32[192,2048]{1,0:T(8,128)S(1)} fusion(bf16[192,2,2048]{2,1,0:T(2,128)(2,1)} %gather.7, pred[192,2]{1,0:T(8,128)(4,1)S(1)} %copy.85, f32[192,2]{1,0:T(8,128)S(1)} %copy.80), kind=kLoop, calls=%fused_computation.52 | loop fusion | flops 2752512 | bytes 3147648 | tf_op jit(solution)/shard_map/reduce_sum | solution.py:177
  (252 shorter events, 66.7 us)
Async XLA Ops:
  6.5 444.9 %copy-start = (bf16[1,512,2048]{2,1,0:T(8,128)(2,1)S(1)}, bf16[1,512,2048]{2,1,0:T(8,128)(2,1)}, u32[]{:S(2)}) copy-start(bf16[1,512,2048]{2,1,0:T(8,128)(2,1)} %param.41) | copy-start | bytes 6291460
  6.5 60.6 %all-gather.6.cloned.1.call-start = ((), (), s32[]{:S(2)}) async-start(), calls=%async_computation.4 | async-start | bytes 1671168 | tf_op jit(solution)/shard_map/all_gather | solution.py:115
  7.3 119.3 %all-gather.8.cloned.1.call-start = ((), (), s32[]{:S(2)}) async-start(), calls=%async_computation.5 | async-start | bytes 1671168 | tf_op jit(solution)/shard_map/all_gather | solution.py:116
  8.0 189.3 %all-gather.10.cloned.1.call-start = ((), (), s32[]{:S(2)}) async-start(), calls=%async_computation.6 | async-start | bytes 3342336 | tf_op jit(solution)/shard_map/all_gather | solution.py:117
  8.7 246.6 %all-gather.12.cloned.1.call-start = ((), (), s32[]{:S(2)}) async-start(), calls=%async_computation.7 | async-start | bytes 1671168 | tf_op jit(solution)/shard_map/all_gather | solution.py:118
  9.3 336.5 %reduce-scatter.3.cloned.1.call-start = ((), (), s32[]{:S(2)}) async-start(), calls=%async_computation.8 | async-start | bytes 2359296 | tf_op jit(solution)/shard_map/reduce_scatter | solution.py:136
  305.3 3.0 copy-start.4
  308.3 1.9 copy-start.6
  310.1 2.2 copy-start.5
  310.1 35.7 %copy-start.1 = (bf16[192,2048]{1,0:T(8,128)(2,1)S(1)}, bf16[192,2048]{1,0:T(8,128)(2,1)}, u32[]{:S(2)}) copy-start(bf16[192,2048]{1,0:T(8,128)(2,1)} %param.34) | copy-start | bytes 2359300
  310.1 132.8 %all-gather.14.cloned.1.call-start = ((), (), s32[]{:S(2)}) async-start(), calls=%async_computation.9 | async-start | bytes 9437184 | tf_op jit(solution)/shard_map/all_gather | solution.py:159
  345.8 1.6 copy-start.3
  345.8 2.1 copy-start.2
  425.8 53.6 %reduce-scatter.5.cloned.1.call-start = ((), (), s32[]{:S(2)}) async-start(), calls=%async_computation.10 | async-start | bytes 9437184 | tf_op jit(solution)/shard_map/reduce_scatter | solution.py:166
  479.4 7.5 %copy-start.7 = (f32[192,2]{0,1:T(2,128)S(1)}, f32[192,2]{0,1:T(2,128)}, u32[]{:S(2)}) copy-start(f32[192,2]{0,1:T(2,128)} %param.38) | copy-start | bytes 4612
  479.4 77.3 %all-to-all-start.1 = ((bf16[16,48,2048]{2,1,0:T(8,128)(2,1)}), bf16[16,48,2048]{2,1,0:T(8,128)(2,1)}, u32[]{:S(2)}, u32[]{:S(2)}) async-start(bf16[16,48,2048]{2,1,0:T(8,128)(2,1)} %bitcast.140), calls=%async_computation.3 | async-start | bytes 6291456 | tf_op jit(solution)/shard_map/all_to_all | solution.py:172
Sparse Core Ops, SparseCore 0:
  10.1 56.9 all-gather.5
  69.9 56.6 all-gather.7
  129.4 67.9 all-gather.9
  200.0 55.2 all-gather.11
  310.3 35.5 reduce-scatter.2
  425.9 16.9 all-gather.13
  463.3 16.0 reduce-scatter.4
where the time goes:
time: 587 us; the launch traced here: 584 us
  waiting for transfers between devices  304 us (52%)
  blocking collectives  76.4 us (13%)
  local copies, waits for them, and re-layouts  59 us (10%)
  matrix products  57.9 us (10%)
  loops' own time  33.4 us (6%)
  other arithmetic  32.2 us (5%)
  between operations  13.8 us (2%)
  starting transfers between devices  7.52 us (1%)
    all_to_all x1, blocking collectives, shards(): lax.all_to_all(outgoing, 'sp', split_axis=0, concat_axis=0, tiled=True)  76.4 us
    all_to_all x1, waiting for transfers between devices, shards(): lax.all_to_all(summed.reshape(experts, capacity, features), 'sp', split_a...  69.6 us
    all_gather x1, waiting for transfers between devices, shards(): lax.all_gather(key_small, 'sp', axis=0, tiled=True)  51.5 us
    all_gather x1, waiting for transfers between devices, shards(): lax.all_gather(value_large, 'sp', axis=0, tiled=True)  48.2 us
    all_gather x1, waiting for transfers between devices, shards(): lax.all_gather(value_small, 'sp', axis=0, tiled=True)  44.8 us
    reduce_scatter x1, waiting for transfers between devices, shards(): lax.psum_scatter(jnp.dot(flattened, weight_rows, preferred_element_type=j...  33.5 us
    another operation x2, loops' own time, advance(): lax.scan(update, carried, (key_blocks, value_blocks, jnp.arange(blocks)))  32.4 us
    all_gather x1, waiting for transfers between devices, shards(): lax.all_gather(key_large, 'sp', axis=0, tiled=True)  20.7 us
  transfers between devices with their start and end apart: 8, of which 8 were waited for; matrix products, arithmetic and copies ran while one was open for 11% of the time, Pallas kernels for 0%

commit v1 on v0

v1 whole, which is shorter than its diff:
```python
import jax
import jax.numpy as jnp
from jax import lax
from jax.experimental import pallas as pl
from jax.experimental.pallas import tpu as pltpu
from jax.sharding import PartitionSpec as P

residual_gain = 8.0**0.25
epsilon = 1e-05
masked_score = -1e30
log2_e = 1.4426950408889634


def layer_norm(values, gain_row):
    average = jnp.mean(values, axis=-1, keepdims=True)
    centred = values - average
    variance = jnp.mean(centred * centred, axis=-1, keepdims=True)
    return centred * lax.rsqrt(variance + epsilon) * gain_row.astype(jnp.float32)


def attention_kernel(
    place, lambda_ref, slope_ref, gain_ref, small_ref, large_ref, block_ref, out_ref, bias, top, total, mixed
):
    step = pl.program_id(0)
    mine = place[0]
    length = small_ref.shape[0]
    rows = block_ref.shape[0]
    small = small_ref.shape[1] // 2
    large = large_ref.shape[1] // 2
    value = out_ref.shape[1] // 2
    small_value = 2 * small
    large_key = small_value + value
    large_value = large_key + 2 * large

    @pl.when(step == 0)
    def _():
        apart = lax.broadcasted_iota(jnp.int32, (rows, length), 0) - lax.broadcasted_iota(
            jnp.int32, (rows, length), 1
        )
        for group in range(2):
            bias[group] = apart.astype(jnp.float32) * (slope_ref[group] * log2_e)
        top[...] = jnp.full(top.shape, masked_score, jnp.float32)
        total[...] = jnp.zeros(total.shape, jnp.float32)
        mixed[...] = jnp.zeros(mixed.shape, jnp.float32)

    def fold(diagonal):
        for group in range(2):
            width = (small, large)[group]
            key_start = (0, large_key)[group]
            value_start = (small_value, large_value)[group]
            query_ref = (small_ref, large_ref)[group]
            values = block_ref[:, value_start : value_start + value]
            away = ((step - mine) * rows).astype(jnp.float32) * (slope_ref[group] * log2_e)
            for part in range(2):
                number = 2 * group + part
                keys = block_ref[:, key_start + part * width : key_start + (part + 1) * width]
                queries = query_ref[:, part * width : (part + 1) * width]
                scores = lax.dot_general(
                    keys, queries, (((1,), (1,)), ((), ())), preferred_element_type=jnp.float32
                )
                scores = scores * (width ** (-0.5) * log2_e) + bias[group]
                if diagonal:
                    seen = lax.broadcasted_iota(jnp.int32, (rows, length), 0)
                    asked = lax.broadcasted_iota(jnp.int32, (rows, length), 1)
                    scores = jnp.where(seen <= asked, scores, masked_score)
                old = top[number]
                new = jnp.maximum(old, jnp.max(scores, axis=0, keepdims=True) + away)
                weights = jnp.exp2(scores - (new - away))
                factor = jnp.exp2(old - new)
                top[number] = new
                total[number] = total[number] * factor + jnp.sum(weights, axis=0, keepdims=True)
                mixed[number] = mixed[number] * factor + lax.dot_general(
                    values,
                    weights.astype(jnp.bfloat16),
                    (((0,), (0,)), ((), ())),
                    preferred_element_type=jnp.float32,
                )

    @pl.when(step < mine)
    def _():
        fold(False)

    @pl.when(step == mine)
    def _():
        fold(True)
        for group in range(2):
            first = mixed[2 * group] / total[2 * group]
            second = mixed[2 * group + 1] / total[2 * group + 1]
            head_out = first - lambda_ref[group] * second
            square = jnp.mean(head_out * head_out, axis=0, keepdims=True)
            head_out = (head_out * lax.rsqrt(square + epsilon)).T
            out_ref[:, group * value : (group + 1) * value] = (
                head_out * gain_ref[...].astype(jnp.float32)
            ).astype(jnp.bfloat16)


def attend(place, lambda_row, slope_row, head_gain, small_queries, large_queries, gathered):
    length = small_queries.shape[0]
    value = head_gain.shape[0]
    columns = gathered.shape[1]
    whole = lambda step, place: (0, 0)
    return pl.pallas_call(
        attention_kernel,
        grid_spec=pltpu.PrefetchScalarGridSpec(
            num_scalar_prefetch=1,
            grid=(gathered.shape[0] // length,),
            in_specs=[
                pl.BlockSpec(memory_space=pltpu.SMEM),
                pl.BlockSpec(memory_space=pltpu.SMEM),
                pl.BlockSpec((1, value), whole),
                pl.BlockSpec(small_queries.shape, whole),
                pl.BlockSpec(large_queries.shape, whole),
                pl.BlockSpec((length, columns), lambda step, place: (jnp.minimum(step, place[0]), 0)),
            ],
            out_specs=pl.BlockSpec((length, 2 * value), whole),
            scratch_shapes=[
                pltpu.VMEM((2, length, length), jnp.float32),
                pltpu.VMEM((4, 1, length), jnp.float32),
                pltpu.VMEM((4, 1, length), jnp.float32),
                pltpu.VMEM((4, value, length), jnp.float32),
            ],
        ),
        out_shape=jax.ShapeDtypeStruct((length, 2 * value), jnp.bfloat16),
        compiler_params=pltpu.CompilerParams(dimension_semantics=("arbitrary",)),
    )(place, lambda_row, slope_row, head_gain.reshape(1, -1), small_queries, large_queries, gathered)


def expert_half(rows, gate, up, down):
    gate_in = jnp.dot(rows, gate, preferred_element_type=jnp.float32)
    upward = jnp.dot(rows, up, preferred_element_type=jnp.float32)
    hidden = (jax.nn.silu(gate_in) * upward).astype(jnp.bfloat16)
    return jnp.dot(hidden, down, preferred_element_type=jnp.float32).astype(jnp.bfloat16)


def shards(
    query_small,
    key_small,
    value_small,
    query_large,
    key_large,
    value_large,
    lambdas,
    slopes,
    head_gain,
    residual,
    out_weight,
    norm_gains,
    routes,
    route_weights,
    gate_weight,
    up_weight,
    down_weight,
):
    length = query_small.shape[0]
    own = jnp.concatenate(
        [array[:, 0] for array in (key_small, value_small, key_large, value_large)], axis=1
    )
    gathered = lax.all_gather(own, "sp", axis=0, tiled=True)
    place = jnp.reshape(lax.axis_index("sp"), (1,)).astype(jnp.int32)
    attended = attend(
        place, lambdas[0], slopes[0], head_gain, query_small[:, 0], query_large[:, 0], gathered
    )
    row_count = length // lax.axis_size("tp")
    core = lax.axis_index("tp")
    swap = ((0, 1), (1, 0))
    halves = attended.reshape(2, row_count, -1)
    kept = jnp.where(core == 0, halves[0], halves[1])
    taken = lax.ppermute(jnp.where(core == 0, halves[1], halves[0]), "tp", swap)
    flattened = jnp.concatenate(
        [jnp.where(core == 0, kept, taken), jnp.where(core == 0, taken, kept)], axis=1
    )
    projected = jnp.dot(flattened, out_weight, preferred_element_type=jnp.float32)
    middle = layer_norm(
        residual_gain * residual.astype(jnp.float32) + projected, norm_gains[0]
    ).astype(jnp.bfloat16)
    experts = lax.axis_size("sp")
    capacity = 4 * row_count // experts
    features = middle.shape[1]
    chosen = routes.reshape(-1)
    matches = (chosen[:, None] == jnp.arange(experts)[None, :]).astype(jnp.int32)
    earlier = jnp.cumsum(matches, axis=0) - matches
    target = chosen * capacity + jnp.sum(earlier * matches, axis=1)
    selector = jnp.any(
        target.reshape(row_count, 2)[None, :, :] == jnp.arange(experts * capacity)[:, None, None],
        axis=2,
    ).astype(jnp.bfloat16)
    outgoing = jnp.dot(selector, middle, preferred_element_type=jnp.float32).astype(jnp.bfloat16)
    outgoing = outgoing.reshape(experts, capacity, features)
    arrived = lax.all_to_all(outgoing, "sp", split_axis=0, concat_axis=0, tiled=True)
    arrived = arrived.reshape(-1, features)
    other = lax.ppermute(arrived, "tp", swap)
    joined_partial = [
        expert_half(rows, gate_weight[0], up_weight[0], down_weight[0]) for rows in (other, arrived)
    ]
    back = lax.ppermute(joined_partial[0], "tp", swap)
    summed = (joined_partial[1].astype(jnp.float32) + back.astype(jnp.float32)).astype(jnp.bfloat16)
    returned = lax.all_to_all(
        summed.reshape(experts, capacity, features), "sp", split_axis=0, concat_axis=0, tiled=True
    )
    expert_out = returned.reshape(experts * capacity, features)
    picked = jnp.take(expert_out, target, axis=0).reshape(row_count, 2, features)
    moe_sum = jnp.sum(route_weights[:, :, None] * picked.astype(jnp.float32), axis=1)
    return layer_norm(residual_gain * middle.astype(jnp.float32) + moe_sum, norm_gains[1]).astype(
        jnp.bfloat16
    )


def solution(mesh):
    placed = (
        P("sp", "tp", None),
        P("sp", "tp", None),
        P("sp", "tp", None),
        P("sp", "tp", None),
        P("sp", "tp", None),
        P("sp", "tp", None),
        P("tp", None),
        P("tp", None),
        P(),
        P(("sp", "tp"), None),
        P(),
        P(),
        P(("sp", "tp"), None),
        P(("sp", "tp"), None),
        P("sp", None, "tp"),
        P("sp", None, "tp"),
        P("sp", "tp", None),
    )
    return jax.shard_map(
        shards, mesh=mesh, in_specs=placed, out_specs=P(("sp", "tp"), None), check_vma=False
    )
```

time: 587 us -> 373 us (0.64)
  waiting for transfers between devices: 304 us -> 185 us
  local copies, waits for them, and re-layouts: 59 us -> 16.6 us
  loops' own time: 33.4 us -> 0 us
  matrix products: 57.9 us -> 29.2 us
  Pallas kernels: 0 us -> 16.4 us
  other arithmetic: 32.2 us -> 16.2 us
  blocking collectives: 76.4 us -> 88.8 us
    all_gather x5 -> x1, waiting for transfers between devices: 182 us -> 106 us  [shards(): gathered = lax.all_gather(own, 'sp', axis=0, tiled=True)]
    reduce_scatter x2 -> x0, waiting for transfers between devices: 49.7 us -> none  [the longest x1 33.5 us: shards(): lax.psum_scatter(jnp.dot(flattened, weight_rows, preferred_element_type=j...]
    another operation x26 -> x0, loops' own time: 33.4 us -> none  [the longest x2 32.4 us: advance(): lax.scan(update, carried, (key_blocks, value_blocks, jnp.arange(blocks)))]
    dot_general x27 -> x5, matrix products: 56.9 us -> 28.1 us  [the longest x2 17.4 us: expert_half(): jnp.dot(hidden, down, preferred_element_type=jnp.float32)]
    pallas_call x0 -> x1, Pallas kernels: none -> 16.4 us  [attend(): pl.pallas_call(attention_kernel, grid_spec=pltpu.PrefetchScalarGridSpec(n...]
    dynamic_slice x24 -> x0, local copies, waits for them, and re-layouts: 16 us -> none  [advance(): lax.scan(update, carried, (key_blocks, value_blocks, jnp.arange(blocks)))]
    all_to_all x1, blocking collectives: 76.4 us -> 88.8 us  [shards(): lax.all_to_all(outgoing, 'sp', split_axis=0, concat_axis=0, tiled=True)]
    reshape x2 -> x0, local copies, waits for them, and re-layouts: 12 us -> none  [advance(): key_blocks = keyset.reshape(blocks, block_rows, head_count, 2, key_width)]
  transfers between devices with their start and end apart: 8 -> 5, of which waited for: 8 -> 5; matrix products, arithmetic and copies ran while one was open for 11% -> 2% of each run, Pallas kernels for 0% -> 0%
where the time goes in v1:
time: 373 us
  waiting for transfers between devices  185 us (50%)
  blocking collectives  88.8 us (24%)
  matrix products  29.2 us (8%)
  local copies, waits for them, and re-layouts  16.6 us (4%)
  Pallas kernels  16.4 us (4%)
  other arithmetic  16.2 us (4%)
  between operations  13.6 us (4%)
  starting transfers between devices  6.75 us (2%)
    all_gather x1, waiting for transfers between devices, shards(): gathered = lax.all_gather(own, 'sp', axis=0, tiled=True)  106 us
    all_to_all x1, blocking collectives, shards(): lax.all_to_all(outgoing, 'sp', split_axis=0, concat_axis=0, tiled=True)  88.8 us
    all_to_all x1, waiting for transfers between devices, shards(): lax.all_to_all(summed.reshape(experts, capacity, features), 'sp', split_a...  72.2 us
    dot_general x2, matrix products, expert_half(): jnp.dot(hidden, down, preferred_element_type=jnp.float32)  17.4 us
    pallas_call x1, Pallas kernels, attend(): pl.pallas_call(attention_kernel, grid_spec=pltpu.PrefetchScalarGridSpec(n...  16.4 us
    gather x2, local copies, waits for them, and re-layouts, shards(): jnp.take(expert_out, target, axis=0).reshape(row_count, 2, features)  11.1 us
    reduce_sum x1, other arithmetic, shards(): jnp.sum(route_weights[:, :, None] * picked.astype(jnp.float32), axis=1)  7.78 us
  transfers between devices with their start and end apart: 5, of which 5 were waited for; matrix products, arithmetic and copies ran while one was open for 2% of the time, Pallas kernels for 0%

profile of v1, /device:TPU:14, one launch (start us, length us, event | category | flops | bytes accessed | tf_op | source)
XLA Modules:
  0.0 372.7 jit_solution(12704563646074936950)
XLA Ops:
  6.5 0.0 copy-start
  6.5 2.1 pad_maximum_fusion
  8.6 0.0 all-gather.2.cloned.1.call-update
  8.6 0.8 copy.33
  9.4 0.1 reshape.118
  9.6 0.1 eq.46
  9.7 0.9 reduce-window.6
  10.6 0.2 slice_reduce_fusion
  10.9 0.1 fusion.26
  11.0 0.1 reduce_sum.61
  11.1 0.1 copy.36
  11.2 0.0 copy-done.5
  11.3 105.8 %all-gather.2.cloned.1.call-done.block_ref = bf16[6144,640]{1,0:T(8,128)(2,1)} async-done(((bf16[384,640]{1,0:T(8,128)(2,1)}), bf16[6144,640]{1,0:T(8,128)(2,1)}) %all-gather.2.cloned.1.call-update) | async-done | bytes 7864336 | tf_op jit(solution)/shard_map/all_gather | solution.py:158
  117.1 16.4 %shard_map.163 = bf16[384,256]{1,0:T(8,128)(2,1)} custom-call(s32[1]{0:T(128)} %bitcast.place, f32[2]{0:T(128)} %bitcast.83, f32[2]{0:T(128)} %bitcast.84, bf16[1,128]{1,0:T(2,128)(2,1)} %bitcast.85, bf16[384,128]{1,0:T(8,128)(2,1)} %bitcast.77, bf16[384,256]{1,0:T(8,128)(2,1)} %bitcast.76, bf16[6144,640]{1,0:T(8,128)(2,1)} %all-gather.2.cloned.1.call-done.block_ref), custom_call_target="tpu_custom_call" | custom-call | tf_op jit(solution)/shard_map/pallas_call | solution.py:102
  133.5 1.0 broadcast_select_fusion.3
  134.4 0.1 collective-permute-start
  134.5 0.2 fusion.12
  134.7 1.1 collective-permute-done
  135.8 1.0 broadcast_select_fusion.2
  136.7 0.0 copy-done.4
  136.8 2.3 fusion.34
  139.1 0.3 multiply_reduce_fusion.2
  139.4 1.1 convolution_convert_fusion.2
  140.6 0.0 copy-start.9
  140.6 88.8 %all_to_all.10 = bf16[16,48,2048]{2,1,0:T(8,128)(2,1)S(1)} all-to-all(bf16[16,48,2048]{2,1,0:T(8,128)(2,1)S(1)} %bitcast.66), channel_id=1, replica_groups=mesh['sp'=16,'tp'=2] {'sp'}, dimensions={0} | all-to-all | bytes 6291456 | tf_op jit(solution)/shard_map/all_to_all | solution.py:189
  229.4 1.7 copy-done.3
  231.0 0.0 collective-permute-start.1
  231.0 5.7 %collective-permute-done.1 = bf16[768,2048]{1,0:T(8,128)(2,1)S(1)} collective-permute-done((bf16[768,2048]{1,0:T(8,128)(2,1)S(1)}, bf16[768,2048]{1,0:T(8,128)(2,1)S(1)}, u32[]{:S(2)}, u32[]{:S(2)}) %collective-permute-start.1) | collective-permute-done | bytes 3145760 | tf_op jit(solution)/shard_map/ppermute | solution.py:191
  236.7 1.7 copy-done.8
  238.4 2.9 fusion.2
  241.3 8.3 %convolution_convert_fusion = bf16[768,2048]{1,0:T(8,128)(2,1)} fusion(bf16[1,512,2048]{2,1,0:T(8,128)(2,1)S(1)} %copy-done, f32[768,512]{1,0:T(8,128)} %fusion.2, bf16[768,2048]{1,0:T(8,128)(2,1)} %copy-done.8, bf16[1,2048,512]{2,1,0:T(8,128)(2,1)} %param.31), kind=kOutput, calls=%fused_computation.2 | convolution fusion | flops 3225157632 | bytes 12058624 | tf_op jit(solution)/shard_map/dot_general | solution.py:132
  249.6 0.1 collective-permute-start.2
  249.7 5.5 %fusion.8 = f32[768,512]{1,0:T(8,128)} fusion(bf16[768,2048]{1,0:T(8,128)(2,1)} %bitcast.68, bf16[1,2048,512]{2,1,0:T(8,128)(2,1)} %param.31), kind=kOutput, calls=%fused_computation.16 | convolution fusion | flops 1610612736 | bytes 6815744 | tf_op jit(solution)/shard_map/dot_general | solution.py:129
  255.2 0.4 collective-permute-done.2
  255.6 9.1 %add_convert_fusion = bf16[768,2048]{1,0:T(8,128)(2,1)} fusion(bf16[768,2048]{1,0:T(8,128)(2,1)} %collective-permute-done.2, bf16[1,512,2048]{2,1,0:T(8,128)(2,1)S(1)} %copy-done, f32[768,512]{1,0:T(8,128)} %fusion.8, bf16[768,2048]{1,0:T(8,128)(2,1)} %bitcast.69, bf16[1,2048,512]{2,1,0:T(8,128)(2,1)} %param.32), kind=kOutput, calls=%fused_computation.1 | convolution fusion | flops 3231449088 | bytes 15204352 | tf_op jit(solution)/shard_map/dot_general | solution.py:132
  264.7 6.5 %all-to-all-start.1 = ((bf16[16,48,2048]{2,1,0:T(8,128)(2,1)}), bf16[16,48,2048]{2,1,0:T(8,128)(2,1)}, u32[]{:S(2)}, u32[]{:S(2)}) async-start(bf16[16,48,2048]{2,1,0:T(8,128)(2,1)} %bitcast.70), calls=%async_computation.1 | async-start | bytes 6291456 | tf_op jit(solution)/shard_map/all_to_all | solution.py:197
  271.3 0.1 copy.38
  271.4 0.1 mul.116
  271.5 0.2 copy.37
  271.7 0.1 copy.32
  271.9 72.2 %all-to-all-done.1 = bf16[16,48,2048]{2,1,0:T(8,128)(2,1)} async-done(((bf16[16,48,2048]{2,1,0:T(8,128)(2,1)}), bf16[16,48,2048]{2,1,0:T(8,128)(2,1)}, u32[]{:S(2)}, u32[]{:S(2)}) %all-to-all-start.1) | async-done | bytes 3145760 | tf_op jit(solution)/shard_map/all_to_all | solution.py:197
  344.0 7.3 %gather_fusion = bf16[384,2048]{1,0:T(8,128)(2,1)} fusion(bf16[768,2048]{1,0:T(8,128)(2,1)} %bitcast.18, s32[1024]{0:T(1024)S(1)} %pad_clamp_fusion), kind=kCustom, calls=%fused_computation | custom fusion | bytes 3147264 | tf_op jit(solution)/shard_map/jit(_take)/gather | solution.py:201
  351.4 3.8 %gather.7 = bf16[192,2,2048]{2,1,0:T(2,128)(2,1)} reshape(bf16[384,2048]{1,0:T(8,128)(2,1)} %gather_fusion) | data formatting | bytes 3145728 | tf_op jit(solution)/shard_map/jit(_take)/gather | solution.py:201
  355.1 7.8 %multiply_reduce_fusion = f32[192,2048]{1,0:T(8,128)S(1)} fusion(bf16[192,2,2048]{2,1,0:T(2,128)(2,1)} %gather.7, pred[192,2]{1,0:T(8,128)(4,1)S(1)} %copy.37, f32[192,2]{1,0:T(8,128)S(1)} %copy.32), kind=kLoop, calls=%fused_computation.5 | loop fusion | flops 2752512 | bytes 3147648 | tf_op jit(solution)/shard_map/reduce_sum | solution.py:202
  362.9 0.0 copy-done.2
  362.9 0.5 fusion.20
  363.4 0.6 multiply_reduce_fusion.1
  364.0 1.8 multiply_convert_fusion
  (25 shorter events, 0.2 us)
Async XLA Ops:
  6.5 234.8 %copy-start = (bf16[1,512,2048]{2,1,0:T(8,128)(2,1)S(1)}, bf16[1,512,2048]{2,1,0:T(8,128)(2,1)}, u32[]{:S(2)}) copy-start(bf16[1,512,2048]{2,1,0:T(8,128)(2,1)} %param.33) | copy-start | bytes 6291460
  6.5 4.7 %copy-start.6 = (s32[192,2]{0,1:T(2,128)S(1)}, s32[192,2]{0,1:T(2,128)}, u32[]{:S(2)}) copy-start(s32[192,2]{0,1:T(2,128)} %param.29) | copy-start | bytes 4612
  6.5 4.7 %copy-start.5 = (bf16[2,2048]{1,0:T(2,128)(2,1)S(1)}, bf16[2,2048]{1,0:T(2,128)(2,1)}, u32[]{:S(2)}) copy-start(bf16[2,2048]{1,0:T(2,128)(2,1)} %param.28) | copy-start | bytes 24580
  6.5 110.5 %all-gather.2.cloned.1.call-start = ((), (), s32[]{:S(2)}) async-start(), calls=%async_computation.2 | async-start | bytes 8355840 | tf_op jit(solution)/shard_map/all_gather | solution.py:158
  117.1 19.7 %copy-start.4 = (bf16[192,2048]{1,0:T(8,128)(2,1)S(1)}, bf16[192,2048]{1,0:T(8,128)(2,1)}, u32[]{:S(2)}) copy-start(bf16[192,2048]{1,0:T(8,128)(2,1)} %param.26) | copy-start | bytes 2359300
  134.4 1.4 collective-permute-start
  139.1 1.5 copy-start.1
  140.6 97.8 %copy-start.9 = (bf16[1,2048,512]{2,1,0:T(8,128)(2,1)S(1)}, bf16[1,2048,512]{2,1,0:T(8,128)(2,1)}, u32[]{:S(2)}) copy-start(bf16[1,2048,512]{2,1,0:T(8,128)(2,1)} %param.32) | copy-start | bytes 6291460
  229.4 1.7 copy-start.3
  231.0 5.7 %collective-permute-start.1 = (bf16[768,2048]{1,0:T(8,128)(2,1)S(1)}, bf16[768,2048]{1,0:T(8,128)(2,1)S(1)}, u32[]{:S(2)}, u32[]{:S(2)}) collective-permute-start(bf16[768,2048]{1,0:T(8,128)(2,1)S(1)} %bitcast.67), channel_id=1, source_target_pairs={{0,1},{1,0},{2,3},{3,2},{4,5},{5,4},{6,7},{7,6},{8,9},{9,8},{10,11... | collective-permute-start | bytes 9437192 | tf_op jit(solution)/shard_map/ppermute | solution.py:191
  236.7 1.7 copy-start.8
  249.6 6.0 %collective-permute-start.2 = (bf16[768,2048]{1,0:T(8,128)(2,1)}, bf16[768,2048]{1,0:T(8,128)(2,1)}, u32[]{:S(2)}, u32[]{:S(2)}) collective-permute-start(bf16[768,2048]{1,0:T(8,128)(2,1)} %convolution_convert_fusion), channel_id=1, source_target_pairs={{0,1},{1,0},{2,3},{3,2},{4,5},{5,4},{6,7},{7,6},{8,9},{9,8},{10,11... | collective-permute-start | bytes 9437192 | tf_op jit(solution)/shard_map/ppermute | solution.py:195
  264.7 7.0 %copy-start.7 = (f32[192,2]{0,1:T(2,128)S(1)}, f32[192,2]{0,1:T(2,128)}, u32[]{:S(2)}) copy-start(f32[192,2]{0,1:T(2,128)} %param.30) | copy-start | bytes 4612
  264.7 79.3 %all-to-all-start.1 = ((bf16[16,48,2048]{2,1,0:T(8,128)(2,1)}), bf16[16,48,2048]{2,1,0:T(8,128)(2,1)}, u32[]{:S(2)}, u32[]{:S(2)}) async-start(bf16[16,48,2048]{2,1,0:T(8,128)(2,1)} %bitcast.70), calls=%async_computation.1 | async-start | bytes 6291456 | tf_op jit(solution)/shard_map/all_to_all | solution.py:197
  355.1 7.8 %copy-start.2 = (f32[192,2048]{1,0:T(8,128)S(1)}, f32[192,2048]{1,0:T(8,128)}, u32[]{:S(2)}) copy-start(f32[192,2048]{1,0:T(8,128)} %copy-done.1) | copy-start | bytes 4718596
Sparse Core Ops, SparseCore 0:
  10.1 106.8 all-gather.1
